TPU v7x, 512 devices: a whole 4x8x8 slice. The times are simulated.
512 devices in a mesh: fs: 64 (over z, y), tp: 8 (over x, core).
Axes of the slice: x: 4, y: 8, z: 8, core: 2. Of those that a mesh axis runs over, the one named last changes fastest.
Arguments:
- tokens: bfloat16 [24576, 2048], P('fs', 'tp'), may hold values from -8 to 8
- w_value: bfloat16 [2048, 1024], P('fs', 'tp'), may hold values from -0.125 to 0.125
- w_gate: bfloat16 [2048, 1024], P('fs', 'tp'), may hold values from -0.125 to 0.125
- conv_kernel: bfloat16 [31, 1024], replicated, may hold values from -1 to 1
- conv_gain: float32 [1024], replicated, may hold values from 0.1 to 1.9
- w_mix_out: bfloat16 [1024, 2048], P('fs', 'tp'), may hold values from -0.1875 to 0.1875
- mix_gain: float32 [2048], replicated, may hold values from 0.1 to 1.9
- w_up: bfloat16 [2048, 8192], P('fs', 'tp'), may hold values from -0.125 to 0.125
- w_down: bfloat16 [8192, 2048], P('tp', 'fs'), may hold values from -0.0625 to 0.0625
- out_gain: float32 [2048], replicated, may hold values from 0.1 to 1.9
Outputs:
- result: bfloat16 [24576, 2048], P('fs', 'tp')
All inputs are finite; a program needn't handle non-finite values.
Results may differ from a plain program's by a relative error of at most 0.013.
Values may be sent and summed in bfloat16 or wider, within the bound.
No kernel may reach another device: no remote copies, remote signals or barrier semaphores. Data moves between devices by JAX's collectives and lax.ppermute only.
A program may use at most 64 MiB of HBM per device.

v0:
```python
import jax
import jax.numpy as jnp
from jax import lax
from jax.sharding import Mesh
from jax.sharding import PartitionSpec as P

WIDTH = 2048
CHANNELS = 1024
KERNEL = 31
LENGTH = 128
FS = ("fs_0", "fs_1")
norm_eps = 1e-05
residual_scale = 2.0**0.5


def joined_along(parts, dim):
    lengths = list(parts.shape[1:])
    lengths[dim] *= parts.shape[0]
    return jnp.moveaxis(parts, 0, dim).reshape(lengths)


def gather_in_order(shard, axes, order):
    parts = shard[None]
    for k in order:
        parts = lax.all_gather(parts, axes[k], axis=0, tiled=True)
    current = [lax.axis_size(axes[k]) for k in reversed(order)]
    parts = parts.reshape(*current, *shard.shape)
    turned = sorted(range(len(order)), key=lambda place: order[len(order) - 1 - place])
    return parts.transpose(*turned, *range(len(order), parts.ndim)).reshape(-1, *shard.shape)


def whole_of(shard, axes, order, dim):
    return joined_along(gather_in_order(shard, axes, order), dim)


def sent_to_all(shard, axis):
    copies = jnp.broadcast_to(shard, (lax.axis_size(axis), *shard.shape))
    return lax.all_to_all(copies, axis, split_axis=0, concat_axis=0, tiled=True)


def gather_directly(shard, axis, dim):
    return joined_along(sent_to_all(shard, axis), dim)


def in_one_piece(arrays, axis, dim, along):
    both = jnp.concatenate(arrays, axis=along)
    out, at, done = (lax.all_gather(both, axis, axis=dim, tiled=True), 0, [])
    for a in arrays:
        done.append(lax.slice_in_dim(out, at, at + a.shape[along], axis=along))
        at += a.shape[along]
    return tuple(done)


def taken_together(shard, axis):
    everything = sent_to_all(shard, axis)
    return jnp.sum(everything, axis=0)


def in_one(arrays, axis):
    ends = [0]
    for a in arrays:
        ends.append(ends[-1] + a.size)
    total = taken_together(jnp.concatenate([a.ravel() for a in arrays]), axis)
    return tuple((total[b:e].reshape(a.shape) for a, b, e in zip(arrays, ends, ends[1:])))


def in_blocks(shard, dim, count):
    lengths = shard.shape
    parts = shard.reshape(*lengths[:dim], count, lengths[dim] // count, *lengths[dim + 1 :])
    return jnp.moveaxis(parts, dim, 0)


def summed_on_arrival(shard, axis, dim):
    count = lax.axis_size(axis)
    parts = lax.all_to_all(in_blocks(shard, dim, count), axis, 0, 0, tiled=True)
    return jnp.sum(parts.astype(jnp.float32), axis=0)


def causal_filter(gated, kernel):
    sequences = gated.shape[0] // LENGTH
    frames = gated.astype(jnp.float32).reshape(sequences, LENGTH, gated.shape[1])
    padded = jnp.pad(frames, ((0, 0), (KERNEL - 1, 0), (0, 0)))
    accumulated = jnp.zeros(frames.shape, jnp.float32)
    for offset in range(KERNEL):
        accumulated = (
            accumulated + kernel[offset].astype(jnp.float32) * padded[:, offset : offset + LENGTH]
        )
    return accumulated.reshape(gated.shape[0], gated.shape[1])


def normalize(values, total_sum, total_sq, entries, gain_vector):
    average = total_sum / entries
    spread = jnp.maximum(total_sq / entries - average * average, 0.0)
    return (values - average[:, None]) * lax.rsqrt(spread[:, None] + norm_eps) * gain_vector


def add_rows(piece, source):
    return jnp.dot(source, piece, preferred_element_type=jnp.float32)


def add_pair(pieces, source):
    first = jnp.dot(source, pieces[0], preferred_element_type=jnp.float32)
    second = jnp.dot(source, pieces[1], preferred_element_type=jnp.float32)
    return (first, second)


def per_device(
    tokens, w_value, w_gate, conv_kernel, conv_gain, w_mix_out, mix_gain, w_up, w_down, out_gain
):
    tp_rank = lax.axis_index("tp")
    width_part = tokens.shape[1]
    channel_part = w_value.shape[1]
    up_collected = lax.all_gather(w_up, FS, axis=0, tiled=True)
    down_collected = whole_of(w_down, FS, (0, 1), 1)
    features = gather_directly(tokens, "tp", 1)
    values_proj, gate_proj = add_pair(in_one_piece((w_value, w_gate), FS, 0, 1), source=features)
    gated = (values_proj * jax.nn.sigmoid(gate_proj)).astype(jnp.bfloat16)
    kernel = lax.dynamic_slice_in_dim(conv_kernel, tp_rank * channel_part, channel_part, 1)
    filtered = causal_filter(gated, kernel)
    channel_sum, channel_sq = in_one((jnp.sum(filtered, 1), jnp.sum(filtered * filtered, 1)), "tp")
    channel_gain = lax.dynamic_slice_in_dim(conv_gain, tp_rank * channel_part, channel_part, 0)
    activated = jax.nn.silu(
        normalize(filtered, channel_sum, channel_sq, CHANNELS, channel_gain)
    ).astype(jnp.bfloat16)
    all_channels = gather_directly(activated, "tp", 1)
    mixed = add_rows(gather_directly(w_mix_out, FS, 0), source=all_channels)
    combined = residual_scale * tokens.astype(jnp.float32) + mixed
    middle_sum, middle_sq = in_one((jnp.sum(combined, 1), jnp.sum(combined * combined, 1)), "tp")
    middle_gain = lax.dynamic_slice_in_dim(mix_gain, tp_rank * width_part, width_part, 0)
    middle = normalize(combined, middle_sum, middle_sq, WIDTH, middle_gain).astype(jnp.bfloat16)
    middle_whole = gather_directly(middle, "tp", 1)
    up_proj = jnp.dot(middle_whole, up_collected, preferred_element_type=jnp.float32)
    hidden = jnp.square(jax.nn.relu(up_proj)).astype(jnp.bfloat16)
    terms = jnp.dot(hidden, down_collected, preferred_element_type=jnp.float32)
    down_sum = summed_on_arrival(terms.astype(jnp.bfloat16), "tp", 1)
    final = residual_scale * middle.astype(jnp.float32) + down_sum
    final_sum, final_sq = in_one((jnp.sum(final, 1), jnp.sum(final * final, 1)), "tp")
    final_gain = lax.dynamic_slice_in_dim(out_gain, tp_rank * width_part, width_part, 0)
    return normalize(final, final_sum, final_sq, WIDTH, final_gain).astype(jnp.bfloat16)


def solution(mesh):
    split = Mesh(mesh.devices.reshape(8, 8, mesh.shape["tp"]), ("fs_0", "fs_1", "tp"))
    in_specs = (
        P(FS, "tp"),
        P(FS, "tp"),
        P(FS, "tp"),
        P(),
        P(),
        P(FS, "tp"),
        P(),
        P(FS, "tp"),
        P("tp", FS),
        P(),
    )
    out_specs = P(FS, "tp")
    return jax.shard_map(
        per_device, mesh=split, in_specs=in_specs, out_specs=out_specs, check_vma=False
    )
```

profile of v0, /device:TPU:1, one launch (start us, length us, event | category | flops | bytes accessed | tf_op | source)
XLA Modules:
  0.0 304.4 jit_solution(7589131715608800212)
XLA Ops:
  6.5 1.4 pad_maximum_fusion
  8.0 27.1 %all-gather = bf16[8192,32]{0,1:T(8,128)(2,1)S(1)} all-gather(bf16[1024,32]{0,1:T(8,128)(2,1)} %param.18), channel_id=2, replica_groups=mesh['fs_0'=8,'fs_1'=8,'tp'=8] {'fs_0'}, dimensions={0}, use_global_device_ids=true | all-gather | bytes 589824 | tf_op jit(solution)/shard_map/all_gather | solution.py:25
  35.1 1.1 copy.78
  36.3 0.7 all-gather.7.cloned.1.call-update
  37.2 1.4 broadcast_in_dim.16
  38.5 10.5 %all-to-all-start = ((bf16[8,384,256]{1,2,0:T(8,128)(2,1)}), bf16[8,384,256]{1,2,0:T(8,128)(2,1)S(1)}, u32[]{:S(2)}, u32[]{:S(2)}) async-start(bf16[8,384,256]{1,2,0:T(8,128)(2,1)} %broadcast_in_dim.16), calls=%async_computation | async-start | bytes 3145728 | tf_op jit(solution)/shard_map/all_to_all | solution.py:38
  49.0 1.0 fusion.102
  50.1 1.1 fusion.103
  51.2 18.4 %all-to-all-done = bf16[8,384,256]{1,2,0:T(8,128)(2,1)S(1)} async-done(((bf16[8,384,256]{1,2,0:T(8,128)(2,1)}), bf16[8,384,256]{1,2,0:T(8,128)(2,1)S(1)}, u32[]{:S(2)}, u32[]{:S(2)}) %all-to-all-start) | async-done | bytes 1572896 | tf_op jit(solution)/shard_map/all_to_all | solution.py:38
  69.6 23.6 %all-gather.5.cloned.1.call-done = bf16[2048,256]{1,0:T(8,128)(2,1)} async-done(((bf16[32,256]{1,0:T(8,128)(2,1)}), bf16[2048,256]{1,0:T(8,128)(2,1)}) %all-gather.5.cloned.1.call-update) | async-done | bytes 1048592 | tf_op jit(solution)/shard_map/all_gather | solution.py:47
  93.2 1.6 fusion.8
  95.5 0.7 fusion.106
  96.3 14.3 %all_to_all.43 = f32[8,1,768]{2,1,0:T(1,128)S(1)} all-to-all(f32[8,1,768]{2,1,0:T(1,128)S(1)} %broadcast_in_dim.17), channel_id=1, replica_groups=mesh['fs_0'=8,'fs_1'=8,'tp'=8] {'tp'}, dimensions={0} | all-to-all | bytes 49152 | tf_op jit(solution)/shard_map/all_to_all | solution.py:38
  110.5 0.9 broadcast_in_dim.19
  111.4 8.6 %all-to-all-start.3 = ((bf16[64,16,256]{2,1,0:T(8,128)(2,1)}), bf16[64,16,256]{2,1,0:T(8,128)(2,1)S(1)}, u32[]{:S(2)}, u32[]{:S(2)}) async-start(bf16[64,16,256]{2,1,0:T(8,128)(2,1)} %broadcast_in_dim.19), calls=%async_computation.3 | async-start | bytes 1048576 | tf_op jit(solution)/shard_map/all_to_all | solution.py:38
  120.0 0.8 dynamic_slice.13
  121.1 22.2 %all-to-all-done.3 = bf16[64,16,256]{2,1,0:T(8,128)(2,1)S(1)} async-done(((bf16[64,16,256]{2,1,0:T(8,128)(2,1)}), bf16[64,16,256]{2,1,0:T(8,128)(2,1)S(1)}, u32[]{:S(2)}, u32[]{:S(2)}) %all-to-all-start.3) | async-done | bytes 524320 | tf_op jit(solution)/shard_map/all_to_all | solution.py:38
  143.5 16.5 %all_to_all.44 = bf16[8,384,128]{1,2,0:T(8,128)(2,1)S(1)} all-to-all(bf16[8,384,128]{1,2,0:T(8,128)(2,1)S(1)} %broadcast_in_dim.18), channel_id=1, replica_groups=mesh['fs_0'=8,'fs_1'=8,'tp'=8] {'tp'}, dimensions={0} | all-to-all | bytes 1572864 | tf_op jit(solution)/shard_map/all_to_all | solution.py:38
  161.1 4.2 %all-to-all-start.4 = ((f32[8,1,768]{2,1,0:T(1,128)}), f32[8,1,768]{2,1,0:T(1,128)S(1)}, u32[]{:S(2)}, u32[]{:S(2)}) async-start(f32[8,1,768]{2,1,0:T(1,128)} %broadcast_in_dim.20), calls=%async_computation.4 | async-start | bytes 49152 | tf_op jit(solution)/shard_map/all_to_all | solution.py:38
  165.3 0.8 dynamic_slice.14
  166.1 3.9 %all-to-all-done.4 = f32[8,1,768]{2,1,0:T(1,128)S(1)} async-done(((f32[8,1,768]{2,1,0:T(1,128)}), f32[8,1,768]{2,1,0:T(1,128)S(1)}, u32[]{:S(2)}, u32[]{:S(2)}) %all-to-all-start.4) | async-done | bytes 24608 | tf_op jit(solution)/shard_map/all_to_all | solution.py:38
  170.2 1.3 broadcast_in_dim.21
  171.5 4.2 %all-to-all-start.5 = ((bf16[8,384,256]{1,2,0:T(8,128)(2,1)}), bf16[8,384,256]{1,2,0:T(8,128)(2,1)S(1)}, u32[]{:S(2)}, u32[]{:S(2)}) async-start(bf16[8,384,256]{1,2,0:T(8,128)(2,1)} %broadcast_in_dim.21), calls=%async_computation.5 | async-start | bytes 3145728 | tf_op jit(solution)/shard_map/all_to_all | solution.py:38
  175.7 6.5 %copy.60 = bf16[8,8,1024,32]{2,3,1,0:T(8,128)(2,1)} copy(bf16[8,8,1024,32]{2,0,1,3:T(8,128)(2,1)} %bitcast.207) | data formatting | bytes 8388608 | tf_op jit(solution)/shard_map/transpose | solution.py:29
  182.2 14.1 %all-to-all-done.5 = bf16[8,384,256]{1,2,0:T(8,128)(2,1)S(1)} async-done(((bf16[8,384,256]{1,2,0:T(8,128)(2,1)}), bf16[8,384,256]{1,2,0:T(8,128)(2,1)S(1)}, u32[]{:S(2)}, u32[]{:S(2)}) %all-to-all-start.5) | async-done | bytes 1572896 | tf_op jit(solution)/shard_map/all_to_all | solution.py:38
  196.3 53.9 %all-gather.7.cloned.1.call-done = bf16[2048,1024]{1,0:T(8,128)(2,1)} async-done(((bf16[32,1024]{1,0:T(8,128)(2,1)}), bf16[2048,1024]{1,0:T(8,128)(2,1)}) %all-gather.7.cloned.1.call-update) | async-done | bytes 4194320 | tf_op jit(solution)/shard_map/all_gather | solution.py:113
  250.2 6.9 %convolution_convert_fusion = bf16[384,2048]{1,0:T(8,128)(2,1)S(1)} fusion(bf16[1024,2048]{0,1:T(8,128)(2,1)} %bitcast.208, bf16[384,2048]{0,1:T(8,128)(2,1)S(1)} %bitcast.211, bf16[2048,1024]{1,0:T(8,128)(2,1)} %all-gather.7.cloned.1.call-done), kind=kOutput, calls=%fused_computation.1 | convolution fusion | flops 3223191552 | bytes 11534336 | tf_op jit(solution)/shard_map/dot_general | solution.py:134
  257.2 29.4 %all_to_all.45 = bf16[8,384,256]{2,1,0:T(8,128)(2,1)S(1)} all-to-all(bf16[8,384,256]{2,1,0:T(8,128)(2,1)S(1)} %bitcast.206), channel_id=1, replica_groups=mesh['fs_0'=8,'fs_1'=8,'tp'=8] {'tp'}, dimensions={0} | all-to-all | bytes 3145728 | tf_op jit(solution)/shard_map/all_to_all | solution.py:75
  287.8 4.3 %all-to-all-start.7 = ((f32[8,1,768]{2,1,0:T(1,128)}), f32[8,1,768]{2,1,0:T(1,128)S(1)}, u32[]{:S(2)}, u32[]{:S(2)}) async-start(f32[8,1,768]{2,1,0:T(1,128)} %broadcast_in_dim.23), calls=%async_computation.7 | async-start | bytes 49152 | tf_op jit(solution)/shard_map/all_to_all | solution.py:38
  292.1 0.8 dynamic_slice.15
  292.9 3.9 %all-to-all-done.7 = f32[8,1,768]{2,1,0:T(1,128)S(1)} async-done(((f32[8,1,768]{2,1,0:T(1,128)}), f32[8,1,768]{2,1,0:T(1,128)S(1)}, u32[]{:S(2)}, u32[]{:S(2)}) %all-to-all-start.7) | async-done | bytes 24608 | tf_op jit(solution)/shard_map/all_to_all | solution.py:38
  297.0 0.8 copy.65
  (37 shorter events, 4.1 us)
Async XLA Ops:
  6.5 30.4 %copy-start.1 = (bf16[384,256]{1,0:T(8,128)(2,1)S(1)}, bf16[384,256]{1,0:T(8,128)(2,1)}, u32[]{:S(2)}) copy-start(bf16[384,256]{1,0:T(8,128)(2,1)} %param.10) | copy-start | bytes 589828
  6.5 86.7 %all-gather.5.cloned.1.call-start = ((), (), s32[]{:S(2)}) async-start(), calls=%async_computation.8 | async-start | bytes 1064960 | tf_op jit(solution)/shard_map/all_gather | solution.py:47
  7.9 167.8 %all-gather.9.cloned.1.call-start = ((), (), s32[]{:S(2)}) async-start(), calls=%async_computation.10 | async-start | bytes 4718592 | tf_op jit(solution)/shard_map/all_gather | solution.py:25
  36.2 214.0 %all-gather.7.cloned.1.call-start = ((), (), s32[]{:S(2)}) async-start(), calls=%async_computation.9 | async-start | bytes 4259840 | tf_op jit(solution)/shard_map/all_gather | solution.py:113
  38.5 31.1 %all-to-all-start = ((bf16[8,384,256]{1,2,0:T(8,128)(2,1)}), bf16[8,384,256]{1,2,0:T(8,128)(2,1)S(1)}, u32[]{:S(2)}, u32[]{:S(2)}) async-start(bf16[8,384,256]{1,2,0:T(8,128)(2,1)} %broadcast_in_dim.16), calls=%async_computation | async-start | bytes 3145728 | tf_op jit(solution)/shard_map/all_to_all | solution.py:38
  93.2 1.6 copy-start
  94.8 15.7 %copy-start.2 = (bf16[16,256]{1,0:T(8,128)(2,1)S(1)}, bf16[16,256]{1,0:T(8,128)(2,1)}, u32[]{:S(2)}) copy-start(bf16[16,256]{1,0:T(8,128)(2,1)} %param.15) | copy-start | bytes 24580
  111.4 32.0 %all-to-all-start.3 = ((bf16[64,16,256]{2,1,0:T(8,128)(2,1)}), bf16[64,16,256]{2,1,0:T(8,128)(2,1)S(1)}, u32[]{:S(2)}, u32[]{:S(2)}) async-start(bf16[64,16,256]{2,1,0:T(8,128)(2,1)} %broadcast_in_dim.19), calls=%async_computation.3 | async-start | bytes 1048576 | tf_op jit(solution)/shard_map/all_to_all | solution.py:38
  161.1 8.9 %all-to-all-start.4 = ((f32[8,1,768]{2,1,0:T(1,128)}), f32[8,1,768]{2,1,0:T(1,128)S(1)}, u32[]{:S(2)}, u32[]{:S(2)}) async-start(f32[8,1,768]{2,1,0:T(1,128)} %broadcast_in_dim.20), calls=%async_computation.4 | async-start | bytes 49152 | tf_op jit(solution)/shard_map/all_to_all | solution.py:38
  171.5 24.8 %all-to-all-start.5 = ((bf16[8,384,256]{1,2,0:T(8,128)(2,1)}), bf16[8,384,256]{1,2,0:T(8,128)(2,1)S(1)}, u32[]{:S(2)}, u32[]{:S(2)}) async-start(bf16[8,384,256]{1,2,0:T(8,128)(2,1)} %broadcast_in_dim.21), calls=%async_computation.5 | async-start | bytes 3145728 | tf_op jit(solution)/shard_map/all_to_all | solution.py:38
  287.8 9.0 %all-to-all-start.7 = ((f32[8,1,768]{2,1,0:T(1,128)}), f32[8,1,768]{2,1,0:T(1,128)S(1)}, u32[]{:S(2)}, u32[]{:S(2)}) async-start(f32[8,1,768]{2,1,0:T(1,128)} %broadcast_in_dim.23), calls=%async_computation.7 | async-start | bytes 49152 | tf_op jit(solution)/shard_map/all_to_all | solution.py:38
Sparse Core Ops, SparseCore 0:
  10.4 82.7 all-gather.4
  95.3 69.8 all-gather.8
  168.3 81.8 all-gather.6
where the time goes:
time: 305 us; the launch traced here: 304 us
  waiting for transfers between devices  141 us (46%)
  blocking collectives  87.3 us (29%)
  starting transfers between devices  31.9 us (10%)
  local copies, waits for them, and re-layouts  16.3 us (5%)
  between operations  13.3 us (4%)
  matrix products  9.49 us (3%)
  other arithmetic  5.24 us (2%)
    all_to_all x5, waiting for transfers between devices, sent_to_all(): return lax.all_to_all(copies, axis, split_axis=0, concat_axis=0, tiled=True)  62.7 us
    all_gather x1, waiting for transfers between devices, per_device(): up_collected = lax.all_gather(w_up, FS, axis=0, tiled=True)  53.9 us
    all_to_all x5, starting transfers between devices, sent_to_all(): return lax.all_to_all(copies, axis, split_axis=0, concat_axis=0, tiled=True)  31.8 us
    all_to_all x2, blocking collectives, sent_to_all(): return lax.all_to_all(copies, axis, split_axis=0, concat_axis=0, tiled=True)  30.7 us
    all_to_all x1, blocking collectives, summed_on_arrival(): parts = lax.all_to_all(in_blocks(shard, dim, count), axis, 0, 0, tiled=True)  29.4 us
    all_gather x1, blocking collectives, gather_in_order(): parts = lax.all_gather(parts, axes[k], axis=0, tiled=True)  27.1 us
    all_gather x1, waiting for transfers between devices, in_one_piece(): out, at, done = (lax.all_gather(both, axis, axis=dim, tiled=True), 0, [])  23.6 us
    dot_general x1, matrix products, per_device(): terms = jnp.dot(hidden, down_collected, preferred_element_type=jnp.float32)  6.89 us
  transfers between devices with their start and end apart: 8, of which 7 were waited for; matrix products, arithmetic and copies ran while one was open for 7% of the time, Pallas kernels for 0%

commit v1 on v0

--- a/solution.py
+++ b/solution.py
@@ -3,6 +3,7 @@
 from jax import lax
 from jax.sharding import Mesh
 from jax.sharding import PartitionSpec as P
+from jax.lax import all_to_all, axis_size
 
 WIDTH = 2048
 CHANNELS = 1024
@@ -110,7 +111,9 @@
     tp_rank = lax.axis_index("tp")
     width_part = tokens.shape[1]
     channel_part = w_value.shape[1]
-    up_collected = lax.all_gather(w_up, FS, axis=0, tiled=True)
+    heard = jnp.stack([w_up for _ in range(axis_size(FS))], axis=0)
+    block_next = all_to_all(heard, FS, 0, 0)
+    up_collected = jnp.concatenate(block_next, axis=0)
     down_collected = whole_of(w_down, FS, (0, 1), 1)
     features = gather_directly(tokens, "tp", 1)
     values_proj, gate_proj = add_pair(in_one_piece((w_value, w_gate), FS, 0, 1), source=features)

time: 305 us -> 440 us (1.44)
  blocking collectives: 87.3 us -> 196 us
  waiting for transfers between devices: 141 us -> 161 us
    all_gather x1, blocking collectives: 27.1 us -> 115 us  [gather_in_order(): parts = lax.all_gather(parts, axes[k], axis=0, tiled=True)]
    all_gather x1, waiting for transfers between devices: 0.01 us -> 66.4 us  [gather_in_order(): parts = lax.all_gather(parts, axes[k], axis=0, tiled=True)]
    all_gather x1 -> x0, waiting for transfers between devices: 53.9 us -> none  [per_device(): up_collected = lax.all_gather(w_up, FS, axis=0, tiled=True)]
    all_gather x1, waiting for transfers between devices: 23.6 us -> 52 us  [in_one_piece(): out, at, done = (lax.all_gather(both, axis, axis=dim, tiled=True), 0, [])]
    all_to_all x2 -> x3, blocking collectives: 30.7 us -> 55.8 us  [sent_to_all(): return lax.all_to_all(copies, axis, split_axis=0, concat_axis=0, tiled=True)]
    all_to_all x5 -> x4, waiting for transfers between devices: 62.7 us -> 42.6 us  [sent_to_all(): return lax.all_to_all(copies, axis, split_axis=0, concat_axis=0, tiled=True)]
    all_to_all x0 -> x1, starting transfers between devices: none -> 5.79 us  [per_device(): block_next = all_to_all(heard, FS, 0, 0)]
    all_to_all x5 -> x4, starting transfers between devices: 31.8 us -> 27.5 us  [sent_to_all(): return lax.all_to_all(copies, axis, split_axis=0, concat_axis=0, tiled=True)]
  transfers between devices with their start and end apart: 8 -> 7, of which waited for: 7 -> 6; matrix products, arithmetic and copies ran while one was open for 7% -> 3% of each run, Pallas kernels for 0% -> 0%
where the time goes in v1:
time: 440 us; the launch traced here: 439 us
  blocking collectives  196 us (45%)
  waiting for transfers between devices  161 us (37%)
  starting transfers between devices  33.3 us (8%)
  local copies, waits for them, and re-layouts  18.4 us (4%)
  between operations  15 us (3%)
  matrix products  9.49 us (2%)
  other arithmetic  5.2 us (1%)
    all_gather x1, blocking collectives, gather_in_order(): parts = lax.all_gather(parts, axes[k], axis=0, tiled=True)  115 us
    all_gather x1, waiting for transfers between devices, gather_in_order(): parts = lax.all_gather(parts, axes[k], axis=0, tiled=True)  66.4 us
    all_to_all x3, blocking collectives, sent_to_all(): return lax.all_to_all(copies, axis, split_axis=0, concat_axis=0, tiled=True)  55.8 us
    all_gather x1, waiting for transfers between devices, in_one_piece(): out, at, done = (lax.all_gather(both, axis, axis=dim, tiled=True), 0, [])  52 us
    all_to_all x4, waiting for transfers between devices, sent_to_all(): return lax.all_to_all(copies, axis, split_axis=0, concat_axis=0, tiled=True)  42.6 us
    all_to_all x4, starting transfers between devices, sent_to_all(): return lax.all_to_all(copies, axis, split_axis=0, concat_axis=0, tiled=True)  27.5 us
    all_to_all x1, blocking collectives, summed_on_arrival(): parts = lax.all_to_all(in_blocks(shard, dim, count), axis, 0, 0, tiled=True)  25.5 us
  transfers between devices with their start and end apart: 7, of which 6 were waited for; matrix products, arithmetic and copies ran while one was open for 3% of the time, Pallas kernels for 0%

profile of v1, /device:TPU:1, one launch (start us, length us, event | category | flops | bytes accessed | tf_op | source)
XLA Modules:
  0.0 438.8 jit_solution(17375884976350513322)
XLA Ops:
  7.4 1.3 pad_maximum_fusion
  8.7 1.1 copy.53
  9.8 1.3 broadcast_in_dim.16
  11.1 10.3 %all-to-all-start = ((bf16[8,384,256]{1,2,0:T(8,128)(2,1)}), bf16[8,384,256]{1,2,0:T(8,128)(2,1)S(1)}, u32[]{:S(2)}, u32[]{:S(2)}) async-start(bf16[8,384,256]{1,2,0:T(8,128)(2,1)} %broadcast_in_dim.16), calls=%async_computation | async-start | bytes 3145728 | tf_op jit(solution)/shard_map/all_to_all | solution.py:39
  21.4 1.0 fusion.102
  22.5 1.1 fusion.103
  23.6 18.4 %all-to-all-done = bf16[8,384,256]{1,2,0:T(8,128)(2,1)S(1)} async-done(((bf16[8,384,256]{1,2,0:T(8,128)(2,1)}), bf16[8,384,256]{1,2,0:T(8,128)(2,1)S(1)}, u32[]{:S(2)}, u32[]{:S(2)}) %all-to-all-start) | async-done | bytes 1572896 | tf_op jit(solution)/shard_map/all_to_all | solution.py:39
  42.0 52.0 %all-gather.4.cloned.1.call-done = bf16[2048,256]{1,0:T(8,128)(2,1)} async-done(((bf16[32,256]{1,0:T(8,128)(2,1)}), bf16[2048,256]{1,0:T(8,128)(2,1)}) %all-gather.4.cloned.1.call-update) | async-done | bytes 1048592 | tf_op jit(solution)/shard_map/all_gather | solution.py:48
  94.1 1.6 fusion.8
  96.3 0.7 fusion.106
  97.1 14.2 %all_to_all.48 = f32[8,1,768]{2,1,0:T(1,128)S(1)} all-to-all(f32[8,1,768]{2,1,0:T(1,128)S(1)} %broadcast_in_dim.17), channel_id=1, replica_groups=mesh['fs_0'=8,'fs_1'=8,'tp'=8] {'tp'}, dimensions={0} | all-to-all | bytes 49152 | tf_op jit(solution)/shard_map/all_to_all | solution.py:39
  111.3 0.8 broadcast_in_dim.19
  112.2 8.6 %all-to-all-start.3 = ((bf16[64,16,256]{2,1,0:T(8,128)(2,1)}), bf16[64,16,256]{2,1,0:T(8,128)(2,1)S(1)}, u32[]{:S(2)}, u32[]{:S(2)}) async-start(bf16[64,16,256]{2,1,0:T(8,128)(2,1)} %broadcast_in_dim.19), calls=%async_computation.3 | async-start | bytes 1048576 | tf_op jit(solution)/shard_map/all_to_all | solution.py:39
  120.8 0.8 dynamic_slice.13
  121.9 16.3 %all-to-all-done.3 = bf16[64,16,256]{2,1,0:T(8,128)(2,1)S(1)} async-done(((bf16[64,16,256]{2,1,0:T(8,128)(2,1)}), bf16[64,16,256]{2,1,0:T(8,128)(2,1)S(1)}, u32[]{:S(2)}, u32[]{:S(2)}) %all-to-all-start.3) | async-done | bytes 524320 | tf_op jit(solution)/shard_map/all_to_all | solution.py:39
  138.2 17.7 %all_to_all.49 = bf16[8,384,128]{1,2,0:T(8,128)(2,1)S(1)} all-to-all(bf16[8,384,128]{1,2,0:T(8,128)(2,1)S(1)} %broadcast_in_dim.18), channel_id=1, replica_groups=mesh['fs_0'=8,'fs_1'=8,'tp'=8] {'tp'}, dimensions={0} | all-to-all | bytes 1572864 | tf_op jit(solution)/shard_map/all_to_all | solution.py:39
  157.1 4.3 all-to-all-start.4
  161.4 0.8 dynamic_slice.14
  162.2 3.9 all-to-all-done.4
  166.4 23.8 %all_to_all.50 = bf16[8,384,256]{1,2,0:T(8,128)(2,1)S(1)} all-to-all(bf16[8,384,256]{1,2,0:T(8,128)(2,1)S(1)} %broadcast_in_dim.21), channel_id=1, replica_groups=mesh['fs_0'=8,'fs_1'=8,'tp'=8] {'tp'}, dimensions={0} | all-to-all | bytes 3145728 | tf_op jit(solution)/shard_map/all_to_all | solution.py:39
  190.3 2.5 stack.2
  192.8 5.8 %all-to-all-start.6 = ((bf16[64,32,1024]{2,1,0:T(8,128)(2,1)}), bf16[64,32,1024]{2,1,0:T(8,128)(2,1)}, u32[]{:S(2)}, u32[]{:S(2)}) async-start(bf16[64,32,1024]{2,1,0:T(8,128)(2,1)} %stack.2), calls=%async_computation.6 | async-start | bytes 8388608 | tf_op jit(solution)/shard_map/all_to_all | solution.py:115
  198.6 115.0 %all-gather = bf16[8192,32]{0,1:T(8,128)(2,1)S(1)} all-gather(bf16[1024,32]{0,1:T(8,128)(2,1)S(1)} %copy-done.2), channel_id=2, replica_groups=mesh['fs_0'=8,'fs_1'=8,'tp'=8] {'fs_0'}, dimensions={0}, use_global_device_ids=true | all-gather | bytes 589824 | tf_op jit(solution)/shard_map/all_gather | solution.py:26
  313.6 1.1 copy.78
  314.8 66.4 %all-gather.6.cloned.1.call-done = bf16[64,1024,32]{1,0,2:T(8,128)(2,1)} async-done(((bf16[8,1024,32]{1,0,2:T(8,128)(2,1)}), bf16[64,1024,32]{1,0,2:T(8,128)(2,1)}) %all-gather.6.cloned.1.call-update) | async-done | bytes 4194320 | tf_op jit(solution)/shard_map/all_gather | solution.py:26
  381.2 6.5 %copy.60 = bf16[8,8,1024,32]{2,3,1,0:T(8,128)(2,1)} copy(bf16[8,8,1024,32]{2,0,1,3:T(8,128)(2,1)} %bitcast.208) | data formatting | bytes 8388608 | tf_op jit(solution)/shard_map/transpose | solution.py:30
  387.7 6.9 %convolution_convert_fusion = bf16[384,2048]{1,0:T(8,128)(2,1)S(1)} fusion(bf16[1024,2048]{0,1:T(8,128)(2,1)} %bitcast.209, bf16[384,2048]{0,1:T(8,128)(2,1)S(1)} %bitcast.212, bf16[2048,1024]{1,0:T(8,128)(2,1)} %bitcast.44), kind=kOutput, calls=%fused_computation.1 | convolution fusion | flops 3223191552 | bytes 11534336 | tf_op jit(solution)/shard_map/dot_general | solution.py:137
  394.7 25.5 %all_to_all.51 = bf16[8,384,256]{2,1,0:T(8,128)(2,1)S(1)} all-to-all(bf16[8,384,256]{2,1,0:T(8,128)(2,1)S(1)} %bitcast.207), channel_id=1, replica_groups=mesh['fs_0'=8,'fs_1'=8,'tp'=8] {'tp'}, dimensions={0} | all-to-all | bytes 3145728 | tf_op jit(solution)/shard_map/all_to_all | solution.py:76
  421.4 4.3 all-to-all-start.8
  425.7 0.8 dynamic_slice.15
  426.4 3.9 all-to-all-done.8
  430.6 0.8 copy.65
  (38 shorter events, 4.1 us)
Async XLA Ops:
  7.4 86.7 %all-gather.4.cloned.1.call-start = ((), (), s32[]{:S(2)}) async-start(), calls=%async_computation.9 | async-start | bytes 1064960 | tf_op jit(solution)/shard_map/all_gather | solution.py:48
  11.1 30.9 %all-to-all-start = ((bf16[8,384,256]{1,2,0:T(8,128)(2,1)}), bf16[8,384,256]{1,2,0:T(8,128)(2,1)S(1)}, u32[]{:S(2)}, u32[]{:S(2)}) async-start(bf16[8,384,256]{1,2,0:T(8,128)(2,1)} %broadcast_in_dim.16), calls=%async_computation | async-start | bytes 3145728 | tf_op jit(solution)/shard_map/all_to_all | solution.py:39
  94.1 1.6 copy-start
  95.7 15.7 %copy-start.3 = (bf16[16,256]{1,0:T(8,128)(2,1)S(1)}, bf16[16,256]{1,0:T(8,128)(2,1)}, u32[]{:S(2)}) copy-start(bf16[16,256]{1,0:T(8,128)(2,1)} %param.15) | copy-start | bytes 24580
  112.2 26.0 %all-to-all-start.3 = ((bf16[64,16,256]{2,1,0:T(8,128)(2,1)}), bf16[64,16,256]{2,1,0:T(8,128)(2,1)S(1)}, u32[]{:S(2)}, u32[]{:S(2)}) async-start(bf16[64,16,256]{2,1,0:T(8,128)(2,1)} %broadcast_in_dim.19), calls=%async_computation.3 | async-start | bytes 1048576 | tf_op jit(solution)/shard_map/all_to_all | solution.py:39
  157.1 9.0 %all-to-all-start.4 = ((f32[8,1,768]{2,1,0:T(1,128)}), f32[8,1,768]{2,1,0:T(1,128)S(1)}, u32[]{:S(2)}, u32[]{:S(2)}) async-start(f32[8,1,768]{2,1,0:T(1,128)} %broadcast_in_dim.20), calls=%async_computation.4 | async-start | bytes 49152 | tf_op jit(solution)/shard_map/all_to_all | solution.py:39
  166.4 23.9 %copy-start.1 = (bf16[32,1024]{1,0:T(8,128)(2,1)S(1)}, bf16[32,1024]{1,0:T(8,128)(2,1)}, u32[]{:S(2)}) copy-start(bf16[32,1024]{1,0:T(8,128)(2,1)} %param.17) | copy-start | bytes 196612
  192.8 5.9 %copy-start.2 = (bf16[1024,32]{0,1:T(8,128)(2,1)S(1)}, bf16[1024,32]{0,1:T(8,128)(2,1)}, u32[]{:S(2)}) copy-start(bf16[1024,32]{0,1:T(8,128)(2,1)} %param.18) | copy-start | bytes 196612
  192.8 194.9 %all-to-all-start.6 = ((bf16[64,32,1024]{2,1,0:T(8,128)(2,1)}), bf16[64,32,1024]{2,1,0:T(8,128)(2,1)}, u32[]{:S(2)}, u32[]{:S(2)}) async-start(bf16[64,32,1024]{2,1,0:T(8,128)(2,1)} %stack.2), calls=%async_computation.6 | async-start | bytes 8388608 | tf_op jit(solution)/shard_map/all_to_all | solution.py:115
  198.6 182.6 %all-gather.6.cloned.1.call-start = ((), (), s32[]{:S(2)}) async-start(), calls=%async_computation.10 | async-start | bytes 4718592 | tf_op jit(solution)/shard_map/all_gather | solution.py:26
  421.4 9.0 %all-to-all-start.8 = ((f32[8,1,768]{2,1,0:T(1,128)}), f32[8,1,768]{2,1,0:T(1,128)S(1)}, u32[]{:S(2)}, u32[]{:S(2)}) async-start(f32[8,1,768]{2,1,0:T(1,128)} %broadcast_in_dim.23), calls=%async_computation.8 | async-start | bytes 49152 | tf_op jit(solution)/shard_map/all_to_all | solution.py:39
Sparse Core Ops, SparseCore 0:
  11.2 82.7 all-gather.3
Sparse Core Ops, SparseCore 1:
  314.8 66.3 all-gather.5
